TPU v7x, 32 devices: a whole 2x2x4 slice. The times are simulated.
32 devices in a mesh: rep: 2 (over x), fs: 4 (over z), tp: 4 (over y, core).
Axes of the slice: x: 2, y: 2, z: 4, core: 2. Of those that a mesh axis runs over, the one named last changes fastest.
Arguments:
- tokens: bfloat16 [8192, 2048], P(('rep', 'fs'), 'tp'), may hold values from -6 to 6
- mix_in_gain: bfloat16 [2048], replicated, may hold values from 0.099609375 to 1.8984375
- bgate_weight: bfloat16 [2048, 2048], P('fs', 'tp'), may hold values from -0.125 to 0.125
- cgate_weight: bfloat16 [2048, 2048], P('fs', 'tp'), may hold values from -0.125 to 0.125
- value_weight: bfloat16 [2048, 2048], P('fs', 'tp'), may hold values from -0.125 to 0.125
- conv_taps: bfloat16 [3, 2048], replicated, may hold values from -3 to 3
- out_weight: bfloat16 [2048, 2048], P('tp', 'fs'), may hold values from -0.41984465 to 0.41984465
- mix_out_gain: bfloat16 [2048], replicated, may hold values from 0.099609375 to 1.8984375
- ffn_in_gain: bfloat16 [2048], replicated, may hold values from 0.099609375 to 1.8984375
- up_weight: bfloat16 [2048, 8192], P('fs', 'tp'), may hold values from -0.125 to 0.125
- down_weight: bfloat16 [8192, 2048], P('tp', 'fs'), may hold values from -0.20992233 to 0.20992233
- ffn_out_gain: bfloat16 [2048], replicated, may hold values from 0.099609375 to 1.8984375
Outputs:
- result: bfloat16 [8192, 2048], P(('rep', 'fs'), 'tp')
All inputs are finite; a program needn't handle non-finite values.
Results may differ from a plain program's by a relative error of at most 0.02.
Values may be sent and summed in bfloat16 or wider, within the bound.
A program may use at most 128 MiB of HBM per device.

v0:
```python
import functools

import jax
import jax.numpy as jnp
from jax import lax
from jax.experimental import pallas as pl
from jax.experimental.pallas import tpu as pltpu
from jax.sharding import PartitionSpec as P

LEN = 256
LANES = 128
AHEAD = 1

epsilon = 1e-06
MESH = pl.DeviceIdType.MESH
F32 = jnp.float32
BF16 = jnp.bfloat16


def at(index, size):
    return pl.ds(pl.multiple_of(index * size, size), size)


def dot(left, right):
    return jnp.dot(left, right, preferred_element_type=F32)


def kernel(
    nfs, ntp, nu, nc, cw,
    tokens, gain1, wb, wc, wv, taps, wo, gain2, gain3, wu, wd, gain4,
    result,
    rows_w, out_w, down_w, tok, normed, part, rs, mix, active, energy,
    recv_z, recv_x, send_r, send_l, send_x, local_sem, tok_local,
    tok_send, tok_recv, rs_send, rs_recv, ag_send, ag_recv, ff_send, ff_recv, en_send, en_recv,
):
    rep, fs, tp = lax.axis_index("rep"), lax.axis_index("fs"), lax.axis_index("tp")
    count, own = tokens.shape
    width = own * ntp
    seqs = count // LEN
    krows = wb.shape[0]
    chan = wb.shape[1]
    ucol = wu.shape[1] // nu
    ocol = wo.shape[1]
    nk = 3 + 1 + nu + nc
    first_down = 4 + nu

    barrier = pltpu.get_barrier_semaphore()
    for step in (1, nfs - 1):
        pl.semaphore_signal(barrier, inc=1, device_id={"fs": lax.rem(fs + step, nfs)}, device_id_type=MESH)
    pl.semaphore_signal(barrier, inc=1, device_id={"rep": 1 - rep}, device_id_type=MESH)
    for step in range(1, ntp):
        pl.semaphore_signal(barrier, inc=1, device_id={"tp": lax.rem(tp + step, ntp)}, device_id_type=MESH)
    pl.semaphore_wait(barrier, 3 + ntp - 1)

    def region(k, s, half):
        if k < 3 or 4 <= k < first_down:
            index = k if k < 3 else k - 1
            if half is None:
                return rows_w.at[index, at(s, krows), :]
            return rows_w.at[index, at(s * 2 + half, krows // 2), :]
        if k == 3:
            r = slice(None) if half is None else at(half, wo.shape[0] // 2)
            return out_w.at[r, at(s, ocol)]
        r = slice(None) if half is None else at(half, wd.shape[0] // 2)
        return down_w.at[k - first_down, r, at(s, cw)]

    def source(k, half):
        if k < 3:
            ref, c = (wb, wc, wv)[k], slice(None)
        elif k == 3:
            ref, c = wo, slice(None)
        elif k < first_down:
            ref, c = wu, pl.ds((k - 4) * ucol, ucol)
        else:
            ref, c = wd, pl.ds((k - first_down) * cw, cw)
        r = slice(None) if half is None else at(half, ref.shape[0] // 2)
        return ref.at[r, c]

    def hop(k, s, src, sems, to):
        return pltpu.make_async_remote_copy(
            src, region(k, s, rep), sems.at[k, s], recv_z.at[k, s],
            device_id={"fs": to}, device_id_type=MESH)

    def right(k, s, src=None):
        return hop(k, s, region(k, s, rep) if src is None else src, send_r, lax.rem(fs + 1, nfs))

    def left(k, s, src=None):
        return hop(k, s, region(k, s, rep) if src is None else src, send_l, lax.rem(fs + nfs - 1, nfs))

    def across(k, s, half):
        return pltpu.make_async_remote_copy(
            region(k, s, half), region(k, s, half), send_x.at[k, s], recv_x.at[k, s],
            device_id={"rep": 1 - rep}, device_id_type=MESH)

    def send_own(k):
        @pl.when(fs < nfs - 1)
        def _():
            right(k, fs, source(k, rep)).start()

        @pl.when(fs > 0)
        def _():
            left(k, fs, source(k, rep)).start()

    def local(k):
        return pltpu.make_async_copy(source(k, None), region(k, fs, None), local_sem.at[k])

    def advance(k):
        if k + AHEAD < nk:
            send_own(k + AHEAD)

        def one(d, carry):
            @pl.when(fs - d >= 0)
            def _():
                s = fs - d
                right(k, s).wait_recv()

                @pl.when(fs < nfs - 1)
                def _():
                    right(k, s).start()

                across(k, s, rep).start()

            @pl.when(fs + d < nfs)
            def _():
                s = fs + d
                left(k, s).wait_recv()

                @pl.when(fs > 0)
                def _():
                    left(k, s).start()

                across(k, s, rep).start()

            return carry

        lax.fori_loop(1, nfs, one, 0)

    def complete(k):
        def one(s, carry):
            @pl.when(s != fs)
            def _():
                across(k, s, 1 - rep).wait_recv()

            return carry

        lax.fori_loop(0, nfs, one, 0)
        local(k).wait()

    def drain(k):
        def one(s, carry):
            @pl.when((s <= fs) & (fs < nfs - 1))
            def _():
                right(k, s).wait_send()

            @pl.when((s >= fs) & (fs > 0))
            def _():
                left(k, s).wait_send()

            @pl.when(s != fs)
            def _():
                across(k, s, rep).wait_send()

            return carry

        lax.fori_loop(0, nfs, one, 0)

    def group(t, src, dst, send, recv):
        return pltpu.make_async_remote_copy(
            src, dst, send, recv,
            device_id={"tp": lax.rem(tp + t, ntp)}, device_id_type=MESH)

    def tok_copy(t):
        mine = tok.at[:, at(tp, own)]
        return group(t, tokens, mine, tok_send.at[t - 1], tok_recv.at[t - 1])

    def rs_copy(t):
        to = lax.rem(tp + t, ntp)
        return group(t, part.at[:, at(to, own)], rs.at[t - 1], rs_send.at[t - 1], rs_recv.at[t - 1])

    def ag_copy(t):
        mine = mix.at[:, at(tp, own)]
        return group(t, mine, mine, ag_send.at[t - 1], ag_recv.at[t - 1])

    block = nfs * cw
    piece = block // ntp

    def ff_copy(t, c):
        to = lax.rem(tp + t, ntp)
        src = part.at[:, at(c * ntp + to, piece)]
        return group(t, src, rs.at[t - 1, :, pl.ds(c * piece, piece)], ff_send.at[t - 1, c], ff_recv.at[t - 1, c])

    def en_copy(t):
        return group(t, energy.at[0], energy.at[t], en_send.at[t - 1], en_recv.at[t - 1])

    def each_seq(fn):
        def one(i, carry):
            fn(at(i, LEN))
            return carry

        lax.fori_loop(0, seqs, one, 0)

    def factor(v):
        return lax.rsqrt(jnp.mean(v * v, axis=-1, keepdims=True) + epsilon)

    send_own(0)
    for t in range(1, ntp):
        tok_copy(t).start()
    own_tok = pltpu.make_async_copy(tokens, tok.at[:, at(tp, own)], tok_local)
    own_tok.start()
    for k in range(1, AHEAD):
        send_own(k)
    for k in range(nk):
        local(k).start()

    advance(0)
    advance(1)
    own_tok.wait()
    for t in range(1, ntp):
        tok_copy(t).wait_recv()

    def norm_tokens(r):
        v = tok[r, :].astype(F32)
        normed[r, :] = (v * factor(v) * gain1[...].astype(F32)).astype(BF16)

    each_seq(norm_tokens)
    advance(2)
    advance(3)
    for k in range(3):
        complete(k)

    own_taps = taps[:, at(tp, chan)].astype(F32)
    position = lax.broadcasted_iota(jnp.int32, (LEN, chan), 0)

    def mixer(r):
        rows = normed[r, :]
        inner = dot(rows, rows_w[1]).astype(BF16).astype(F32) * dot(rows, rows_w[2]).astype(BF16).astype(F32)
        before = jnp.where(position == 0, 0.0, pltpu.roll(inner, 1, 0))
        after = jnp.where(position == LEN - 1, 0.0, pltpu.roll(inner, LEN - 1, 0))
        conv = own_taps[0:1] * before + own_taps[1:2] * inner + own_taps[2:3] * after
        outer = dot(rows, rows_w[0]).astype(BF16).astype(F32)
        active[r, 0:chan] = (outer * conv).astype(BF16)

    each_seq(mixer)
    advance(4)
    complete(3)

    def project(r):
        part[r, :] = dot(active[r, 0:chan], out_w[...]).astype(BF16)

    each_seq(project)
    for t in range(1, ntp):
        rs_copy(t).start()
    done = 5
    for k in range(done, min(first_down, nk)):
        advance(k)
    for t in range(1, ntp):
        rs_copy(t).wait_recv()

    def add_mix(r):
        total = part[r, at(tp, own)].astype(F32)
        for t in range(1, ntp):
            total = total + rs[t - 1, r, :].astype(F32)
        mix[r, at(tp, own)] = total.astype(BF16)

    each_seq(add_mix)
    for t in range(1, ntp):
        ag_copy(t).start()
    early = max(nc - 2, 0)
    for c in range(early):
        advance(first_down + c)
    for k in range(4, first_down):
        complete(k)
    for t in range(1, ntp):
        ag_copy(t).wait_recv()

    def second(r):
        m = mix[r, :].astype(F32)
        res = (tok[r, :].astype(F32) + m * factor(m) * gain2[...].astype(F32)).astype(BF16)
        tok[r, :] = res
        res = res.astype(F32)
        rows = (res * factor(res) * gain3[...].astype(F32)).astype(BF16)
        for u in range(nu):
            lifted = jnp.maximum(dot(rows, rows_w[3 + u]), 0.0)
            active[r, pl.ds(u * ucol, ucol)] = (lifted * lifted).astype(BF16)

    for t in range(1, ntp):
        tok_copy(t).wait_send()
        rs_copy(t).wait_send()
    each_seq(second)

    for c in range(nc):
        if early <= c + 1 < nc:
            advance(first_down + c + 1)
        if c == 0 and early == 0:
            advance(first_down)
        complete(first_down + c)

        def down(r):
            part[r, pl.ds(c * block, block)] = dot(active[r, :], down_w[c]).astype(BF16)

        each_seq(down)
        for t in range(1, ntp):
            ff_copy(t, c).start()

    for k in range(nk):
        drain(k)
    for t in range(1, ntp):
        ag_copy(t).wait_send()
        for c in range(nc):
            ff_copy(t, c).wait_recv()

    def own_ffn(r):
        pieces = [part[r, at(c * ntp + tp, piece)] for c in range(nc)]
        total = (pieces[0] if nc == 1 else jnp.concatenate(pieces, axis=1)).astype(F32)
        for t in range(1, ntp):
            total = total + rs[t - 1, r, :].astype(F32)
        return total

    def measure(r):
        total = own_ffn(r)
        square = jnp.sum(total * total, axis=1, keepdims=True)
        flat = jnp.transpose(jnp.broadcast_to(square, (LEN, LANES)))
        energy[0, :, r] = flat[0:8, :]

    each_seq(measure)
    for t in range(1, ntp):
        en_copy(t).start()
    for t in range(1, ntp):
        en_copy(t).wait_recv()
    own_gain = gain4[:, at(tp, own)].astype(F32)

    def close(r):
        total = own_ffn(r)
        flat = energy[0, :, r]
        for t in range(1, ntp):
            flat = flat + energy[t, :, r]
        tall = jnp.transpose(jnp.concatenate([flat] * (LANES // 8), axis=0))
        scale = lax.rsqrt(tall[:, 0:1] / width + epsilon)
        result[r, :] = (tok[r, at(tp, own)].astype(F32) + total * scale * own_gain).astype(BF16)

    each_seq(close)
    for t in range(1, ntp):
        en_copy(t).wait_send()
        for c in range(nc):
            ff_copy(t, c).wait_send()


def solution(mesh):
    nfs, ntp = mesh.shape["fs"], mesh.shape["tp"]
    assert mesh.shape["rep"] == 2

    def body(tokens, gain1, wb, wc, wv, taps, wo, gain2, gain3, wu, wd, gain4):
        count, own = tokens.shape
        width, chan, hidden = own * ntp, wb.shape[1], wu.shape[1]
        ucol = chan
        nu = hidden // ucol
        cw = min(LANES, wd.shape[1])
        nc = wd.shape[1] // cw
        nk = 4 + nu + nc
        vm, anyw = pl.BlockSpec(memory_space=pltpu.VMEM), pl.BlockSpec(memory_space=pl.ANY)
        dma = pltpu.SemaphoreType.DMA
        peers = ntp - 1
        return pl.pallas_call(
            functools.partial(kernel, nfs, ntp, nu, nc, cw),
            out_shape=jax.ShapeDtypeStruct((count, own), BF16),
            in_specs=[anyw, vm, anyw, anyw, anyw, vm, anyw, vm, vm, anyw, anyw, vm],
            out_specs=vm,
            scratch_shapes=[
                pltpu.VMEM((3 + nu, width, chan), BF16),
                pltpu.VMEM((chan, width), BF16),
                pltpu.VMEM((nc, hidden, nfs * cw), BF16),
                pltpu.VMEM((count, width), BF16),
                pltpu.VMEM((count, width), BF16),
                pltpu.VMEM((count, width), BF16),
                pltpu.VMEM((peers, count, own), BF16),
                pltpu.VMEM((count, width), BF16),
                pltpu.VMEM((count, hidden), BF16),
                pltpu.VMEM((ntp, 8, count), F32),
                dma((nk, nfs)), dma((nk, nfs)), dma((nk, nfs)), dma((nk, nfs)), dma((nk, nfs)),
                dma((nk,)), dma,
                dma((peers,)), dma((peers,)), dma((peers,)), dma((peers,)),
                dma((peers,)), dma((peers,)), dma((peers, nc)), dma((peers, nc)),
                dma((peers,)), dma((peers,)),
            ],
            compiler_params=pltpu.CompilerParams(
                collective_id=0, has_side_effects=True, vmem_limit_bytes=64000000),
            name="layer",
        )(tokens, gain1[None], wb, wc, wv, taps, wo, gain2[None], gain3[None], wu, wd, gain4[None])

    placed = (
        P(("rep", "fs"), "tp"), P(), P("fs", "tp"), P("fs", "tp"), P("fs", "tp"), P(), P("tp", "fs"),
        P(), P(), P("fs", "tp"), P("tp", "fs"), P(),
    )
    return jax.shard_map(
        body, mesh=mesh, in_specs=placed, out_specs=P(("rep", "fs"), "tp"), check_vma=False
    )
```

profile of v0, /device:TPU:0, one launch (start us, length us, event | category | flops | bytes accessed | tf_op | source)
XLA Modules:
  0.0 256.1 jit_solution(12055334470951717921)
XLA Ops:
  0.0 1.3 broadcast_in_dim.12.gain1
  1.3 1.3 broadcast_in_dim.13.gain2
  2.6 1.3 broadcast_in_dim.14.gain3
  3.9 1.3 broadcast_in_dim.15.gain4
  5.1 248.7 %layer.1 = bf16[1024,512]{1,0:T(8,128)(2,1)} custom-call(bf16[1024,512]{1,0:T(8,128)(2,1)} %tokens.1, bf16[1,2048]{1,0:T(2,128)(2,1)} %broadcast_in_dim.12.gain1, bf16[512,512]{1,0:T(8,128)(2,1)} %wb.1, bf16[512,512]{1,0:T(8,128)(2,1)} %wc.1, bf16[512,512]{1,0:T(8,128)(2,1)} %wv.1, bf16[3,2048]{1,0:T(4,128)(2,1)} %taps.1, bf16[512,512]{1,0:T(8,128)(2,1)} %wo.1, ...), custom_call_target="tpu_custom_call" | custom-call | tf_op jit(solution)/shard_map/layer/pallas_call | solution.py:363
  253.8 2.3 copy.14
where the time goes:
time: 256 us
  Pallas kernels  249 us (97%)
  local copies, waits for them, and re-layouts  7.41 us (3%)
    pallas_call x1, Pallas kernels, body(): pl.pallas_call(functools.partial(kernel, nfs, ntp, nu, nc, cw), out_shape...  249 us

commit v1 on v0

v1 whole, which is shorter than its diff:
```python
import functools

import jax
import jax.numpy as jnp
from jax import lax
from jax.experimental import pallas as pl
from jax.experimental.pallas import tpu as pltpu
from jax.sharding import PartitionSpec as P

LEN = 256
LANES = 128
DOWN_BOTH = 2

epsilon = 1e-06
MESH = pl.DeviceIdType.MESH
F32 = jnp.float32
BF16 = jnp.bfloat16


def at(index, size):
    return pl.ds(pl.multiple_of(index * size, size), size)


def dot(left, right):
    return jnp.dot(left, right, preferred_element_type=F32)


def loop(low, high, fn):
    def one(i, carry):
        fn(i)
        return carry

    lax.fori_loop(low, high, one, 0)


def kernel(
    nfs, ntp, nu, nc, cw,
    tokens, gain1, wb, wc, wv, taps, wo, gain2, gain3, wu, wd, gain4,
    result,
    rows_w, out_w, down_w, big, active, land, pair, rs, acc, resid, fpart, fpair, frs, energy,
    recv_z, recv_x, send_r, send_l, send_x, local_sem, tok_local,
    ag_ys, ag_ds, ag_recv, land_send, land_recv,
    pair_send, pair_recv, rs_send, rs_recv, en_send, en_recv,
    fp_send, fp_recv, fr_send, fr_recv, back_send, back_recv,
):
    rep, fs, tp = lax.axis_index("rep"), lax.axis_index("fs"), lax.axis_index("tp")
    ny = ntp // 2
    core, y = lax.rem(tp, 2), tp // 2
    sibling = tp + 1 - 2 * core
    count, own = tokens.shape
    width = own * ntp
    seqs = count // LEN
    krows, chan = wb.shape
    hidden = wu.shape[1]
    ucol = hidden // nu
    ocol = wo.shape[1]
    block = nfs * cw
    piece = block // ntp
    odd = lax.rem(fs, 2)
    worker = jnp.where(fs < nfs // 2, odd, 1 - odd) == 1
    partner = fs + 1 - 2 * odd
    end = (fs == 0) | (fs == nfs - 1)

    barrier = pltpu.get_barrier_semaphore()
    for step in (1, nfs - 1):
        pl.semaphore_signal(barrier, inc=1, device_id={"fs": lax.rem(fs + step, nfs)}, device_id_type=MESH)
    pl.semaphore_signal(barrier, inc=1, device_id={"rep": 1 - rep}, device_id_type=MESH)
    for step in range(1, ntp):
        pl.semaphore_signal(barrier, inc=1, device_id={"tp": lax.rem(tp + step, ntp)}, device_id_type=MESH)
    pl.semaphore_wait(barrier, 3 + ntp - 1)

    def slot(kind, j):
        return {"mix": j, "out": 3, "up": 4 + j, "down": 4 + nu + j}[kind]

    def ends(kind):
        return (0, nfs - 1) if kind in ("mix", "out") else (1, nfs - 2)

    def region(kind, j, s, half):
        if kind in ("mix", "up"):
            index = j if kind == "mix" else 3 + j
            if half is None:
                return rows_w.at[index, at(s, krows), :]
            return rows_w.at[index, at(s * 2 + half, krows // 2), :]
        if kind == "out":
            r = slice(None) if half is None else at(half, wo.shape[0] // 2)
            return out_w.at[r, at(s, ocol)]
        r = slice(None) if half is None else at(half, wd.shape[0] // 2)
        return down_w.at[j, r, at(s, cw)]

    def source(kind, j, half):
        if kind == "mix":
            ref, c = (wb, wc, wv)[j], slice(None)
        elif kind == "out":
            ref, c = wo, slice(None)
        elif kind == "up":
            ref, c = wu, at(j, ucol)
        else:
            ref, c = wd, at(j, cw)
        r = slice(None) if half is None else at(half, ref.shape[0] // 2)
        return ref.at[r, c]

    def hop(kind, j, s, mine, sems, to):
        k = slot(kind, j)
        src = source(kind, j, rep) if mine else region(kind, j, s, rep)
        return pltpu.make_async_remote_copy(
            src, region(kind, j, s, rep), sems.at[k, s], recv_z.at[k, s],
            device_id={"fs": to}, device_id_type=MESH)

    def right(kind, j, s, mine=False):
        return hop(kind, j, s, mine, send_r, lax.rem(fs + 1, nfs))

    def left(kind, j, s, mine=False):
        return hop(kind, j, s, mine, send_l, lax.rem(fs + nfs - 1, nfs))

    def across(kind, j, s, half):
        k = slot(kind, j)
        return pltpu.make_async_remote_copy(
            region(kind, j, s, half), region(kind, j, s, half), send_x.at[k, s], recv_x.at[k, s],
            device_id={"rep": 1 - rep}, device_id_type=MESH)

    def extra(kind, j):
        k = slot(kind, j)
        to = jnp.where(fs == 0, 1, nfs - 2)
        return pltpu.make_async_remote_copy(
            source(kind, j, 1 - rep), region(kind, j, fs, 1 - rep), send_x.at[k, fs], recv_x.at[k, fs],
            device_id={"fs": to}, device_id_type=MESH)

    def both(kind, j):
        return j < DOWN_BOTH if kind == "down" else True

    def crosses(kind, j, s):
        near = ((s == 0) & (fs == 1)) | ((s == nfs - 1) & (fs == nfs - 2))
        keep = jnp.logical_not(near & both(kind, j)) & (s != fs)
        return keep if kind in ("mix", "out") else keep & worker

    def send_own(kind, j):
        low, high = ends(kind)

        @pl.when(fs < high)
        def _():
            right(kind, j, fs, True).start()

        @pl.when(fs > low)
        def _():
            left(kind, j, fs, True).start()

        @pl.when(end & both(kind, j))
        def _():
            extra(kind, j).start()

    def local(kind, j):
        return pltpu.make_async_copy(source(kind, j, None), region(kind, j, fs, None), local_sem.at[slot(kind, j)])

    def relay(kind, j):
        low, high = ends(kind)
        inside = (fs >= low) & (fs <= high)

        def one(d):
            @pl.when((fs - d >= 0) & inside)
            def _():
                s = fs - d
                right(kind, j, s).wait_recv()

                @pl.when(fs < high)
                def _():
                    right(kind, j, s).start()

                @pl.when(crosses(kind, j, s))
                def _():
                    across(kind, j, s, rep).start()

            @pl.when((fs + d < nfs) & inside)
            def _():
                s = fs + d
                left(kind, j, s).wait_recv()

                @pl.when(fs > low)
                def _():
                    left(kind, j, s).start()

                @pl.when(crosses(kind, j, s))
                def _():
                    across(kind, j, s, rep).start()

        loop(1, nfs, one)

    def complete(kind, j):
        def one(s):
            @pl.when(s != fs)
            def _():
                across(kind, j, s, 1 - rep).wait_recv()

        loop(0, nfs, one)
        local(kind, j).wait()

    def drain(kind, j):
        low, high = ends(kind)

        def one(s):
            @pl.when((s <= fs) & (fs < high))
            def _():
                right(kind, j, s).wait_send()

            @pl.when((s >= fs) & (fs > low))
            def _():
                left(kind, j, s).wait_send()

            inside = (fs >= low) & (fs <= high)

            @pl.when(crosses(kind, j, s) & inside)
            def _():
                across(kind, j, s, rep).wait_send()

        loop(0, nfs, one)

        @pl.when(end & both(kind, j))
        def _():
            extra(kind, j).wait_send()

    def group(to, src, dst, send, recv):
        return pltpu.make_async_remote_copy(
            src, dst, send, recv, device_id={"tp": to}, device_id_type=MESH)

    def up_y(t):
        return lax.rem(y + t, ny) * 2 + core

    def down_y(t):
        return lax.rem(y + ny - t, ny) * 2 + core

    def gathered(j, i, who):
        return big.at[min(j, 1), at(i, LEN), at(who, own)]

    def ag_y(j, i, t):
        src = tokens.at[at(i, LEN), :] if j == 2 else gathered(j, i, tp)
        return group(up_y(t), src, gathered(j, i, tp), ag_ys.at[j, i, t - 1], ag_recv.at[j, i, tp])

    def ag_pair(j, i):
        src = tokens.at[at(i, LEN), :] if j == 2 else gathered(j, i, tp)
        return group(sibling, src, gathered(j, i, tp), ag_ds.at[j, i, 0], ag_recv.at[j, i, tp])

    def ag_relay(j, i, t):
        who = down_y(t)
        return group(sibling, gathered(j, i, who), gathered(j, i, who), ag_ds.at[j, i, t], ag_recv.at[j, i, who])

    def ag_start(j, i):
        for t in range(1, ny):
            ag_y(j, i, t).start()
        ag_pair(j, i).start()

    def ag_pass(j, i):
        for t in range(1, ny):
            ag_relay(j, i, t).wait_recv()
            ag_relay(j, i, t).start()

    def ag_finish(j, i):
        for t in range(ny):
            who = lax.rem(y + t, ny) * 2 + 1 - core
            group(sibling, gathered(j, i, who), gathered(j, i, who), ag_ds.at[j, i, 0], ag_recv.at[j, i, who]).wait_recv()

    def ag_drain(j, i):
        for t in range(1, ny):
            ag_y(j, i, t).wait_send()
            ag_relay(j, i, t).wait_send()
        ag_pair(j, i).wait_send()

    def hand(i):
        return pltpu.make_async_remote_copy(
            land.at[at(i, LEN), :], land.at[at(i, LEN), :], land_send.at[i], land_recv.at[i],
            device_id={"fs": partner}, device_id_type=MESH)

    def pair_copy(i, b):
        src = active.at[1, at(i, LEN), at(2 * b + 1 - core, own)]
        return group(sibling, src, pair.at[b, at(i, LEN), :], pair_send.at[i, b], pair_recv.at[i, b])

    def rs_copy(i, t):
        src = pair.at[lax.rem(y + t, ny), at(i, LEN), :]
        return group(up_y(t), src, rs.at[t - 1, at(i, LEN), :], rs_send.at[i, t - 1], rs_recv.at[i, t - 1])

    def en_copy(stage, i, t):
        return group(
            lax.rem(tp + t, ntp), energy.at[stage, 0, i], energy.at[stage, t, i],
            en_send.at[stage, i, t - 1], en_recv.at[stage, i, t - 1])

    def en_put(stage, i, values):
        square = jnp.sum(values * values, axis=1, keepdims=True)
        flat = jnp.transpose(jnp.broadcast_to(square, (LEN, LANES)))
        energy[stage, 0, i] = flat[0:8, :]
        for t in range(1, ntp):
            en_copy(stage, i, t).start()

    def en_get(stage, i):
        for t in range(1, ntp):
            en_copy(stage, i, t).wait_recv()
        flat = energy[stage, 0, i]
        for t in range(1, ntp):
            flat = flat + energy[stage, t, i]
        tall = jnp.transpose(jnp.concatenate([flat] * (LANES // 8), axis=0))
        return lax.rsqrt(tall[:, 0:1] / width + epsilon)

    def fp_copy(c, j, i):
        return group(
            sibling, fpart.at[lax.rem(c, 2), j, :, 1 - core, at(i, LEN), :], fpair.at[j, c, :, at(i, LEN), :],
            fp_send.at[j, c, i], fp_recv.at[j, c, i])

    def fr_copy(c, i, t):
        src = fpair.at[0, c, lax.rem(y + t, ny), at(i, LEN), :]
        return group(up_y(t), src, frs.at[t - 1, c, at(i, LEN), :], fr_send.at[c, i, t - 1], fr_recv.at[c, i, t - 1])

    def back(c, i):
        return pltpu.make_async_remote_copy(
            fpair.at[1, c, :, at(i, LEN), :], fpair.at[0, c, :, at(i, LEN), :], back_send.at[c, i], back_recv.at[c, i],
            device_id={"fs": partner}, device_id_type=MESH)

    send_own("mix", 0)
    loop(0, seqs, lambda i: ag_start(2, i))
    own_tok = pltpu.make_async_copy(tokens, big.at[1, :, at(tp, own)], tok_local)
    own_tok.start()
    send_own("mix", 1)
    for k in range(3):
        local("mix", k).start()
    local("out", 0).start()

    @pl.when(worker)
    def _():
        loop(0, nu, lambda j: local("up", j).start())
        loop(0, nc, lambda j: local("down", j).start())

    relay("mix", 0)
    send_own("mix", 2)
    loop(0, seqs, lambda i: ag_pass(2, i))
    relay("mix", 1)
    send_own("out", 0)
    own_tok.wait()

    def norm_tokens(i):
        ag_finish(2, i)
        r = at(i, LEN)
        v = big[1, r, :].astype(F32)
        factor = lax.rsqrt(jnp.mean(v * v, axis=-1, keepdims=True) + epsilon)
        big[0, r, :] = (v * factor * gain1[...].astype(F32)).astype(BF16)

    loop(0, seqs, norm_tokens)
    relay("mix", 2)
    send_own("up", 0)
    for k in range(3):
        complete("mix", k)

    own_taps = taps[:, at(tp, chan)].astype(F32)
    position = lax.broadcasted_iota(jnp.int32, (LEN, chan), 0)

    def mixer(i):
        r = at(i, LEN)
        rows = big[0, r, :]
        inner = dot(rows, rows_w[1]).astype(BF16).astype(F32) * dot(rows, rows_w[2]).astype(BF16).astype(F32)
        before = jnp.where(position == 0, 0.0, pltpu.roll(inner, 1, 0))
        after = jnp.where(position == LEN - 1, 0.0, pltpu.roll(inner, LEN - 1, 0))
        conv = own_taps[0:1] * before + own_taps[1:2] * inner + own_taps[2:3] * after
        outer = dot(rows, rows_w[0]).astype(BF16).astype(F32)
        active[0, r, 0:chan] = (outer * conv).astype(BF16)

        @pl.when(i == seqs // 2)
        def _():
            relay("out", 0)
            send_own("up", min(1, nu - 1)) if nu > 1 else None

    loop(0, seqs, mixer)
    complete("out", 0)

    def project(i):
        r = at(i, LEN)

        @pl.when(i < seqs)
        def _():
            active[1, r, 0:width] = dot(active[0, r, 0:chan], out_w[...]).astype(BF16)
            for b in range(ny):
                pair_copy(i, b).start()

        @pl.when(i > 0)
        def _():
            last = i - 1
            r = at(last, LEN)
            for b in range(ny):
                pair_copy(last, b).wait_recv()
                total = active[1, r, at(2 * b + core, own)].astype(F32) + pair[b, r, :].astype(F32)
                pair[b, r, :] = total.astype(BF16)
            for t in range(1, ny):
                rs_copy(last, t).start()

    loop(0, seqs + 1, project)
    loop(0, seqs, lambda i: ag_drain(2, i))

    own_gain2 = gain2[:, at(tp, own)].astype(F32)
    own_gain3 = gain3[:, at(tp, own)].astype(F32)

    def mixed_sum(i):
        r = at(i, LEN)
        total = pair[y, r, :].astype(F32)
        for t in range(1, ny):
            rs_copy(i, t).wait_recv()
            total = total + rs[t - 1, r, :].astype(F32)
        acc[r, :] = total
        en_put(0, i, total)

    def add_resid(i):
        r = at(i, LEN)
        scale = en_get(0, i)
        res = (big[1, r, at(tp, own)].astype(F32) + acc[r, :] * scale * own_gain2).astype(BF16)
        resid[r, :] = res
        en_put(1, i, res.astype(F32))

    def normalise(i):
        r = at(i, LEN)
        rows = (resid[r, :].astype(F32) * en_get(1, i) * own_gain3).astype(BF16)

        @pl.when(worker)
        def _():
            big[0, r, at(tp, own)] = rows
            ag_start(0, i)

        @pl.when(jnp.logical_not(worker))
        def _():
            land[r, :] = rows
            hand(i).start()

    first = min(2, nu)

    def exchange(step):
        @pl.when(step < nu)
        def _():
            @pl.when(step + first < nu)
            def _():
                send_own("up", step + first)

            @pl.when(step == nu - 1)
            def _():
                send_own("down", 0)

            relay("up", step)

        @pl.when(step < seqs)
        def _():
            mixed_sum(step)

        @pl.when((step >= 1) & (step < seqs + 1))
        def _():
            add_resid(step - 1)

        @pl.when((step >= 2) & (step < seqs + 2))
        def _():
            normalise(step - 2)

        @pl.when((step >= 3) & (step < seqs + 3) & worker)
        def _():
            ag_pass(0, step - 3)

    loop(0, max(seqs + 3, nu), exchange)
    for i in range(seqs):
        for b in range(ny):
            pair_copy(i, b).wait_send()

    def sum_pair(c, j, i):
        r = at(i, LEN)
        fp_copy(c, j, i).wait_recv()
        for b in range(ny):
            total = fpart[lax.rem(c, 2), j, b, core, r, :].astype(F32) + fpair[j, c, b, r, :].astype(F32)
            fpair[j, c, b, r, :] = total.astype(BF16)

    def fr_start(c, i):
        for t in range(1, ny):
            fr_copy(c, i, t).start()

    @pl.when(jnp.logical_not(worker))
    def _():
        loop(1, nc, lambda c: send_own("down", c))

        def returned(c):
            def one(i):
                back(c, i).wait_recv()
                fr_start(c, i)

            loop(0, seqs, one)

        loop(0, nc, returned)

    @pl.when(worker)
    def _():
        loop(0, nu, lambda j: complete("up", j))

        def lift(j, i):
            ag_finish(j, i)
            r = at(i, LEN)
            rows = big[j, r, :]
            for u in range(nu):
                lifted = jnp.maximum(dot(rows, rows_w[3 + u]), 0.0)
                active[j, r, pl.ds(u * ucol, ucol)] = (lifted * lifted).astype(BF16)

        early = min(nc, seqs // 2)

        def pump(c):
            @pl.when(c + 1 < nc)
            def _():
                send_own("down", c + 1)

            relay("down", c)

        def own_rows(i):
            lift(0, i)
            hand(i).wait_recv()
            r = at(i, LEN)
            big[1, r, at(tp, own)] = land[r, :]
            ag_start(1, i)

            @pl.when(i > 0)
            def _():
                ag_pass(1, i - 1)

            @pl.when((lax.rem(i, 2) == 1) & (i // 2 < early))
            def _():
                pump(i // 2)

        loop(0, seqs, own_rows)
        ag_pass(1, seqs - 1)

        def partner_rows(i):
            lift(1, i)
            if early < nc:
                @pl.when(i == seqs // 2)
                def _():
                    pump(early)

        loop(0, seqs, partner_rows)
        ready = min(early + 1, nc)
        lag = 2

        def chunk(c):
            @pl.when((c + 1 >= ready) & (c + 1 < nc))
            def _():
                pump(c + 1)

            complete("down", c)

            def unit(n):
                @pl.when(n < 2 * seqs)
                def _():
                    j, i = 1 - n // seqs, lax.rem(n, seqs)
                    r = at(i, LEN)

                    @pl.when(c >= 2)
                    def _():
                        fp_copy(c - 2, j, i).wait_send()

                    product = dot(active[j, r, 0:hidden], down_w[c]).astype(BF16)
                    for b in range(ny):
                        for half in range(2):
                            lane = (2 * b + half) * piece
                            fpart[lax.rem(c, 2), j, b, half, r, :] = product[:, lane:lane + piece]
                    fp_copy(c, j, i).start()

                @pl.when(n >= lag)
                def _():
                    m = n - lag
                    j, i = 1 - m // seqs, lax.rem(m, seqs)
                    sum_pair(c, j, i)

                    @pl.when(j == 0)
                    def _():
                        fr_start(c, i)

                    @pl.when(j == 1)
                    def _():
                        back(c, i).start()

            loop(0, 2 * seqs + lag, unit)

        loop(0, nc, chunk)

    own_gain4 = gain4[:, at(tp, own)].astype(F32)

    def close(step):
        @pl.when(step < seqs)
        def _():
            r = at(step, LEN)
            parts = []
            for c in range(nc):
                total = fpair[0, c, y, r, :].astype(F32)
                for t in range(1, ny):
                    fr_copy(c, step, t).wait_recv()
                    total = total + frs[t - 1, c, r, :].astype(F32)
                parts.append(total)
            total = parts[0] if nc == 1 else jnp.concatenate(parts, axis=1)
            acc[r, :] = total
            en_put(2, step, total)

        @pl.when(step > 0)
        def _():
            r = at(step - 1, LEN)
            scale = en_get(2, step - 1)
            result[r, :] = (resid[r, :].astype(F32) + acc[r, :] * scale * own_gain4).astype(BF16)

    loop(0, seqs + 1, close)

    for k in range(3):
        drain("mix", k)
    drain("out", 0)
    loop(0, nu, lambda j: drain("up", j))
    loop(0, nc, lambda j: drain("down", j))

    def finish(i):
        for t in range(1, ny):
            rs_copy(i, t).wait_send()
            loop(0, nc, lambda c: fr_copy(c, i, t).wait_send())
        for stage in range(3):
            for t in range(1, ntp):
                en_copy(stage, i, t).wait_send()

        @pl.when(worker)
        def _():
            ag_drain(0, i)
            ag_drain(1, i)
            for j in range(2):
                loop(max(nc - 2, 0), nc, lambda c: fp_copy(c, j, i).wait_send())
            loop(0, nc, lambda c: back(c, i).wait_send())

        @pl.when(jnp.logical_not(worker))
        def _():
            hand(i).wait_send()

    loop(0, seqs, finish)


def solution(mesh):
    nfs, ntp = mesh.shape["fs"], mesh.shape["tp"]
    assert mesh.shape["rep"] == 2 and nfs % 2 == 0 and nfs >= 4 and ntp % 2 == 0

    def body(tokens, gain1, wb, wc, wv, taps, wo, gain2, gain3, wu, wd, gain4):
        count, own = tokens.shape
        width, chan, hidden = own * ntp, wb.shape[1], wu.shape[1]
        nu = hidden // chan
        cw = min(LANES, wd.shape[1])
        nc = wd.shape[1] // cw
        nk = 4 + nu + nc
        ny, seqs = ntp // 2, count // LEN
        piece = nfs * cw // ntp
        vm, anyw = pl.BlockSpec(memory_space=pltpu.VMEM), pl.BlockSpec(memory_space=pl.ANY)
        dma = pltpu.SemaphoreType.DMA
        return pl.pallas_call(
            functools.partial(kernel, nfs, ntp, nu, nc, cw),
            out_shape=jax.ShapeDtypeStruct((count, own), BF16),
            in_specs=[anyw, vm, anyw, anyw, anyw, vm, anyw, vm, vm, anyw, anyw, vm],
            out_specs=vm,
            scratch_shapes=[
                pltpu.VMEM((3 + nu, width, chan), BF16),
                pltpu.VMEM((chan, width), BF16),
                pltpu.VMEM((nc, hidden, nfs * cw), BF16),
                pltpu.VMEM((2, count, width), BF16),
                pltpu.VMEM((2, count, max(hidden, width)), BF16),
                pltpu.VMEM((count, own), BF16),
                pltpu.VMEM((ny, count, own), BF16),
                pltpu.VMEM((ny - 1, count, own), BF16),
                pltpu.VMEM((count, own), F32),
                pltpu.VMEM((count, own), BF16),
                pltpu.VMEM((2, 2, ny, 2, count, piece), BF16),
                pltpu.VMEM((2, nc, ny, count, piece), BF16),
                pltpu.VMEM((ny - 1, nc, count, piece), BF16),
                pltpu.VMEM((3, ntp, seqs, 8, LEN), F32),
                dma((nk, nfs)), dma((nk, nfs)), dma((nk, nfs)), dma((nk, nfs)), dma((nk, nfs)),
                dma((nk,)), dma,
                dma((3, seqs, ny - 1)), dma((3, seqs, ny)), dma((3, seqs, ntp)), dma((seqs,)), dma((seqs,)),
                dma((seqs, ny)), dma((seqs, ny)), dma((seqs, ny - 1)), dma((seqs, ny - 1)),
                dma((3, seqs, ntp - 1)), dma((3, seqs, ntp - 1)),
                dma((2, nc, seqs)), dma((2, nc, seqs)), dma((nc, seqs, ny - 1)), dma((nc, seqs, ny - 1)),
                dma((nc, seqs)), dma((nc, seqs)),
            ],
            compiler_params=pltpu.CompilerParams(
                collective_id=0, has_side_effects=True, vmem_limit_bytes=66000000),
            name="layer",
        )(tokens, gain1[None], wb, wc, wv, taps, wo, gain2[None], gain3[None], wu, wd, gain4[None])

    placed = (
        P(("rep", "fs"), "tp"), P(), P("fs", "tp"), P("fs", "tp"), P("fs", "tp"), P(), P("tp", "fs"),
        P(), P(), P("fs", "tp"), P("tp", "fs"), P(),
    )
    return jax.shard_map(
        body, mesh=mesh, in_specs=placed, out_specs=P(("rep", "fs"), "tp"), check_vma=False
    )
```

time: 256 us -> 270 us (1.055)
  Pallas kernels: 249 us -> 263 us
    pallas_call x1, Pallas kernels: 249 us -> 263 us  [body(): pl.pallas_call(functools.partial(kernel, nfs, ntp, nu, nc, cw), out_shape...]
where the time goes in v1:
time: 270 us
  Pallas kernels  263 us (97%)
  local copies, waits for them, and re-layouts  7.41 us (3%)
    pallas_call x1, Pallas kernels, body(): pl.pallas_call(functools.partial(kernel, nfs, ntp, nu, nc, cw), out_shape...  263 us

profile of v1, /device:TPU:0, one launch (start us, length us, event | category | flops | bytes accessed | tf_op | source)
XLA Modules:
  0.0 269.9 jit_solution(8687102959170543979)
XLA Ops:
  0.0 1.3 broadcast_in_dim.12.gain1
  1.3 1.3 broadcast_in_dim.13.gain2
  2.6 1.3 broadcast_in_dim.14.gain3
  3.9 1.3 broadcast_in_dim.15.gain4
  5.1 262.5 %layer.1 = bf16[1024,512]{1,0:T(8,128)(2,1)} custom-call(bf16[1024,512]{1,0:T(8,128)(2,1)} %tokens.1, bf16[1,2048]{1,0:T(2,128)(2,1)} %broadcast_in_dim.12.gain1, bf16[512,512]{1,0:T(8,128)(2,1)} %wb.1, bf16[512,512]{1,0:T(8,128)(2,1)} %wc.1, bf16[512,512]{1,0:T(8,128)(2,1)} %wv.1, bf16[3,2048]{1,0:T(4,128)(2,1)} %taps.1, bf16[512,512]{1,0:T(8,128)(2,1)} %wo.1, ...), custom_call_target="tpu_custom_call" | custom-call | tf_op jit(solution)/shard_map/layer/pallas_call | solution.py:646
  267.7 2.3 copy.14

commit v2 on v1

--- a/solution.py
+++ b/solution.py
@@ -25,6 +25,14 @@
     return jnp.dot(left, right, preferred_element_type=F32)
 
 
+def row(v):
+    return v.astype(F32).reshape(1, v.shape[0])
+
+
+def early_chunks(nc):
+    return min(2, nc - 1)
+
+
 def loop(low, high, fn):
     def one(i, carry):
         fn(i)
@@ -37,11 +45,11 @@
     nfs, ntp, nu, nc, cw,
     tokens, gain1, wb, wc, wv, taps, wo, gain2, gain3, wu, wd, gain4,
     result,
-    rows_w, out_w, down_w, big, active, land, pair, rs, acc, resid, fpart, fpair, frs, energy,
+    rows_w, out_w, down_w, big, active, land, pair, rs, acc, resid, fpart, fpair, frs, fsum, energy,
     recv_z, recv_x, send_r, send_l, send_x, local_sem, tok_local,
     ag_ys, ag_ds, ag_recv, land_send, land_recv,
     pair_send, pair_recv, rs_send, rs_recv, en_send, en_recv,
-    fp_send, fp_recv, fr_send, fr_recv, back_send, back_recv,
+    fp_send, fp_recv, fr_send, fr_recv, back_send, back_recv, fs_send, fs_recv,
 ):
     rep, fs, tp = lax.axis_index("rep"), lax.axis_index("fs"), lax.axis_index("tp")
     ny = ntp // 2
@@ -54,6 +62,8 @@
     hidden = wu.shape[1]
     ucol = hidden // nu
     ocol = wo.shape[1]
+    nk = 4 + nu + nc
+    n_early = early_chunks(nc)
     block = nfs * cw
     piece = block // ntp
     odd = lax.rem(fs, 2)
@@ -118,11 +128,11 @@
             region(kind, j, s, half), region(kind, j, s, half), send_x.at[k, s], recv_x.at[k, s],
             device_id={"rep": 1 - rep}, device_id_type=MESH)
 
-    def extra(kind, j):
+    def extra(kind, j, src):
         k = slot(kind, j)
         to = jnp.where(fs == 0, 1, nfs - 2)
         return pltpu.make_async_remote_copy(
-            source(kind, j, 1 - rep), region(kind, j, fs, 1 - rep), send_x.at[k, fs], recv_x.at[k, fs],
+            src, region(kind, j, fs, 1 - rep), send_x.at[k, fs], recv_x.at[k, fs],
             device_id={"fs": to}, device_id_type=MESH)
 
     def both(kind, j):
@@ -146,17 +156,20 @@
 
         @pl.when(end & both(kind, j))
         def _():
-            extra(kind, j).start()
+            extra(kind, j, source(kind, j, 1 - rep)).start()
 
     def local(kind, j):
         return pltpu.make_async_copy(source(kind, j, None), region(kind, j, fs, None), local_sem.at[slot(kind, j)])
 
-    def relay(kind, j):
+    def relay(kind, j, first, last, mid=True, out=True):
         low, high = ends(kind)
         inside = (fs >= low) & (fs <= high)
+        lower = fs < nfs // 2
+        from_left = inside & ((lower & out) | (jnp.logical_not(lower) & mid))
+        from_right = inside & ((lower & mid) | (jnp.logical_not(lower) & out))
 
         def one(d):
-            @pl.when((fs - d >= 0) & inside)
+            @pl.when((fs - d >= 0) & from_left)
             def _():
                 s = fs - d
                 right(kind, j, s).wait_recv()
@@ -169,7 +182,7 @@
                 def _():
                     across(kind, j, s, rep).start()
 
-            @pl.when((fs + d < nfs) & inside)
+            @pl.when((fs + d < nfs) & from_right)
             def _():
                 s = fs + d
                 left(kind, j, s).wait_recv()
@@ -182,7 +195,7 @@
                 def _():
                     across(kind, j, s, rep).start()
 
-        loop(1, nfs, one)
+        loop(first, last, one)
 
     def complete(kind, j):
         def one(s):
@@ -215,7 +228,7 @@
 
         @pl.when(end & both(kind, j))
         def _():
-            extra(kind, j).wait_send()
+            extra(kind, j, region(kind, j, fs, 1 - rep)).wait_send()
 
     def group(to, src, dst, send, recv):
         return pltpu.make_async_remote_copy(
@@ -299,7 +312,7 @@
 
     def fp_copy(c, j, i):
         return group(
-            sibling, fpart.at[lax.rem(c, 2), j, :, 1 - core, at(i, LEN), :], fpair.at[j, c, :, at(i, LEN), :],
+            sibling, fpart.at[c, j, :, 1 - core, at(i, LEN), :], fpair.at[j, c, :, at(i, LEN), :],
             fp_send.at[j, c, i], fp_recv.at[j, c, i])
 
     def fr_copy(c, i, t):
@@ -309,6 +322,87 @@
     def back(c, i):
         return pltpu.make_async_remote_copy(
             fpair.at[1, c, :, at(i, LEN), :], fpair.at[0, c, :, at(i, LEN), :], back_send.at[c, i], back_recv.at[c, i],
+            device_id={"fs": partner}, device_id_type=MESH)
+
+    def send_at(k):
+        @pl.when(k == 2)
+        def _():
+            send_own("mix", 2)
+
+        @pl.when(k == 3)
+        def _():
+            send_own("out", 0)
+
+        @pl.when((k >= 4) & (k < 4 + nu))
+        def _():
+            send_own("up", k - 4)
+
+        @pl.when((k >= 4 + nu) & (k < 4 + nu + nc))
+        def _():
+            send_own("down", k - 4 - nu)
+
+    def relay_at(k, first, last, mid, out):
+        @pl.when(k < 3)
+        def _():
+            relay("mix", k, first, last, mid, out)
+
+        @pl.when(k == 3)
+        def _():
+            relay("out", 0, first, last, mid, out)
+
+        @pl.when((k >= 4) & (k < 4 + nu))
+        def _():
+            relay("up", k - 4, first, last, mid, out)
+
+        @pl.when((k >= 4 + nu) & (k < nk))
+        def _():
+            relay("down", k - 4 - nu, first, last, mid, out)
+
+    def take(q):
+        @pl.when(lax.rem(q, 2) == 1)
+        def _():
+            relay_at((q + 1) // 2, 1, 2, True, False)
+
+        @pl.when(lax.rem(q, 2) == 0)
+        def _():
+            relay_at(q // 2, 1, 2, q == 0, True)
+            send_at(q // 2 + 2 + jnp.where(q >= 8, 1, 0))
+
+            @pl.when(q == 6)
+            def _():
+                send_at(6)
+
+            @pl.when(q >= 2)
+            def _():
+                relay_at(q // 2 - 1, 2, nfs, True, True)
+
+    def takes(low, high):
+        @pl.when(worker)
+        def _():
+            with jax.named_scope("take"):
+                loop(low, high, take)
+
+    def outer_mix(*parts):
+        @pl.when(jnp.logical_not(worker))
+        def _():
+            for d, k in parts:
+                kind, j = ("mix", k) if k < 3 else ("out", 0)
+                with jax.named_scope("relay"):
+                    relay(kind, j, d, d + 1 if d < 3 else nfs)
+
+    def send_outer(low, high):
+        @pl.when(jnp.logical_not(worker))
+        def _():
+            loop(4 + low, 4 + min(high, nu + nc), send_at)
+
+    def fs_copy(c, i, t):
+        src = fpair.at[1, c, lax.rem(y + t, ny), at(i, LEN), :]
+        dst = fsum.at[t - 1, c - n_early, at(i, LEN), :]
+        return group(up_y(t), src, dst, fs_send.at[c, i, t - 1], fs_recv.at[c, i, t - 1])
+
+    def back_own(c, i):
+        return pltpu.make_async_remote_copy(
+            fpair.at[1, c, y, at(i, LEN), :], fpair.at[0, c, y, at(i, LEN), :], back_send.at[c, i], back_recv.at[c, i],
             device_id={"fs": partner}, device_id_type=MESH)
 
     send_own("mix", 0)
@@ -316,6 +410,12 @@
     own_tok = pltpu.make_async_copy(tokens, big.at[1, :, at(tp, own)], tok_local)
     own_tok.start()
     send_own("mix", 1)
+
+    @pl.when(jnp.logical_not(worker))
+    def _():
+        send_own("mix", 2)
+        send_own("out", 0)
+
     for k in range(3):
         local("mix", k).start()
     local("out", 0).start()
@@ -325,11 +425,14 @@
         loop(0, nu, lambda j: local("up", j).start())
         loop(0, nc, lambda j: local("down", j).start())
 
-    relay("mix", 0)
-    send_own("mix", 2)
-    loop(0, seqs, lambda i: ag_pass(2, i))
-    relay("mix", 1)
-    send_own("out", 0)
+    takes(0, 3)
+    outer_mix((1, 0), (1, 1), (2, 0), (1, 2))
+    takes(3, 4)
+    with jax.named_scope("tok_pass"):
+        loop(0, seqs, lambda i: ag_pass(2, i))
+    takes(4, 5)
+    outer_mix((2, 1), (3, 0), (1, 3))
+    send_outer(0, 2)
     own_tok.wait()
 
     def norm_tokens(i):
@@ -337,13 +440,18 @@
         r = at(i, LEN)
         v = big[1, r, :].astype(F32)
         factor = lax.rsqrt(jnp.mean(v * v, axis=-1, keepdims=True) + epsilon)
-        big[0, r, :] = (v * factor * gain1[...].astype(F32)).astype(BF16)
-
-    loop(0, seqs, norm_tokens)
-    relay("mix", 2)
-    send_own("up", 0)
-    for k in range(3):
-        complete("mix", k)
+        big[0, r, :] = (v * factor * row(gain1[...])).astype(BF16)
+
+    with jax.named_scope("norm"):
+        loop(0, seqs, norm_tokens)
+    takes(5, 7)
+    outer_mix((2, 2), (3, 1), (2, 3))
+    send_outer(2, nu)
+    outer_mix((3, 2), (3, 3))
+    send_outer(nu, nu + nc)
+    with jax.named_scope("mix_wait"):
+        for k in range(3):
+            complete("mix", k)
 
     own_taps = taps[:, at(tp, chan)].astype(F32)
     position = lax.broadcasted_iota(jnp.int32, (LEN, chan), 0)
@@ -360,11 +468,14 @@
 
         @pl.when(i == seqs // 2)
         def _():
-            relay("out", 0)
-            send_own("up", min(1, nu - 1)) if nu > 1 else None
-
-    loop(0, seqs, mixer)
-    complete("out", 0)
+            takes(8, 9)
+
+    with jax.named_scope("mixer"):
+        loop(0, seqs, mixer)
+    takes(7, 8)
+    takes(9, 10)
+    with jax.named_scope("out_wait"):
+        complete("out", 0)
 
     def project(i):
         r = at(i, LEN)
@@ -386,11 +497,13 @@
             for t in range(1, ny):
                 rs_copy(last, t).start()
 
-    loop(0, seqs + 1, project)
+    with jax.named_scope("project"):
+        loop(0, seqs + 1, project)
+    takes(10, 11)
     loop(0, seqs, lambda i: ag_drain(2, i))
 
-    own_gain2 = gain2[:, at(tp, own)].astype(F32)
-    own_gain3 = gain3[:, at(tp, own)].astype(F32)
+    own_gain2 = row(gain2[at(tp, own)])
+    own_gain3 = row(gain3[at(tp, own)])
 
     def mixed_sum(i):
         r = at(i, LEN)
@@ -422,47 +535,73 @@
             land[r, :] = rows
             hand(i).start()
 
-    first = min(2, nu)
+    def lift(j, i):
+        ag_finish(j, i)
+        r = at(i, LEN)
+        rows = big[j, r, :]
+        for u in range(nu):
+            lifted = jnp.maximum(dot(rows, rows_w[3 + u]), 0.0)
+            active[j, r, pl.ds(u * ucol, ucol)] = (lifted * lifted).astype(BF16)
 
     def exchange(step):
-        @pl.when(step < nu)
-        def _():
-            @pl.when(step + first < nu)
-            def _():
-                send_own("up", step + first)
-
-            @pl.when(step == nu - 1)
-            def _():
-                send_own("down", 0)
-
-            relay("up", step)
+        @pl.when(step <= seqs)
+        def _():
+            takes(11 + step, 12 + step)
 
         @pl.when(step < seqs)
         def _():
-            mixed_sum(step)
-
-        @pl.when((step >= 1) & (step < seqs + 1))
-        def _():
-            add_resid(step - 1)
-
-        @pl.when((step >= 2) & (step < seqs + 2))
-        def _():
-            normalise(step - 2)
-
-        @pl.when((step >= 3) & (step < seqs + 3) & worker)
-        def _():
-            ag_pass(0, step - 3)
-
-    loop(0, max(seqs + 3, nu), exchange)
-    for i in range(seqs):
-        for b in range(ny):
-            pair_copy(i, b).wait_send()
+            with jax.named_scope("mixed_sum"):
+                mixed_sum(step)
+            for b in range(ny):
+                pair_copy(step, b).wait_send()
+
+        @pl.when((step >= seqs) & (step < 2 * seqs))
+        def _():
+            with jax.named_scope("add_resid"):
+                add_resid(step - seqs)
+
+        @pl.when(step >= 2 * seqs)
+        def _():
+            with jax.named_scope("normalise"):
+                normalise(step - 2 * seqs)
+
+        @pl.when(step < 3)
+        def _():
+            drain("mix", step)
+
+    def spread(step):
+        takes(taken + step, taken + step + 1)
+
+        @pl.when(step < seqs)
+        def _():
+            with jax.named_scope("ag_pass0"):
+                ag_pass(0, step)
+
+        @pl.when(step == 1)
+        def _():
+            with jax.named_scope("up_wait"):
+                loop(0, nu, lambda j: complete("up", j))
+
+        @pl.when(step >= 1)
+        def _():
+            with jax.named_scope("lift0"):
+                lift(0, step - 1)
+
+    loop(0, 3 * seqs, exchange)
+    taken = 12 + seqs
+    drain("out", 0)
+
+    @pl.when(worker)
+    def _():
+        loop(0, seqs + 1, spread)
+
+    taken += seqs + 1
 
     def sum_pair(c, j, i):
         r = at(i, LEN)
         fp_copy(c, j, i).wait_recv()
         for b in range(ny):
-            total = fpart[lax.rem(c, 2), j, b, core, r, :].astype(F32) + fpair[j, c, b, r, :].astype(F32)
+            total = fpart[c, j, b, core, r, :].astype(F32) + fpair[j, c, b, r, :].astype(F32)
             fpair[j, c, b, r, :] = total.astype(BF16)
 
     def fr_start(c, i):
@@ -471,7 +610,9 @@
 
     @pl.when(jnp.logical_not(worker))
     def _():
-        loop(1, nc, lambda c: send_own("down", c))
+        loop(0, nu, lambda j: drain("up", j))
+
+        frs[:, n_early:] = jnp.zeros((ny - 1, nc - n_early, count, piece), BF16)
 
         def returned(c):
             def one(i):
@@ -480,101 +621,121 @@
 
             loop(0, seqs, one)
 
-        loop(0, nc, returned)
+        with jax.named_scope("returned"):
+            loop(0, n_early, returned)
 
     @pl.when(worker)
     def _():
-        loop(0, nu, lambda j: complete("up", j))
-
-        def lift(j, i):
-            ag_finish(j, i)
+        lag = 2
+        total = 2 * nk + 1
+
+        def unit(c, j, i):
             r = at(i, LEN)
-            rows = big[j, r, :]
-            for u in range(nu):
-                lifted = jnp.maximum(dot(rows, rows_w[3 + u]), 0.0)
-                active[j, r, pl.ds(u * ucol, ucol)] = (lifted * lifted).astype(BF16)
-
-        early = min(nc, seqs // 2)
-
-        def pump(c):
-            @pl.when(c + 1 < nc)
-            def _():
-                send_own("down", c + 1)
-
-            relay("down", c)
-
-        def own_rows(i):
-            lift(0, i)
-            hand(i).wait_recv()
-            r = at(i, LEN)
-            big[1, r, at(tp, own)] = land[r, :]
-            ag_start(1, i)
-
-            @pl.when(i > 0)
-            def _():
-                ag_pass(1, i - 1)
-
-            @pl.when((lax.rem(i, 2) == 1) & (i // 2 < early))
-            def _():
-                pump(i // 2)
-
-        loop(0, seqs, own_rows)
-        ag_pass(1, seqs - 1)
-
-        def partner_rows(i):
-            lift(1, i)
-            if early < nc:
-                @pl.when(i == seqs // 2)
+            product = dot(active[j, r, 0:hidden], down_w[c]).astype(BF16)
+            for b in range(ny):
+                for odd_ in range(2):
+                    lane = (2 * b + odd_) * piece
+                    fpart[c, j, b, odd_, r, :] = product[:, lane:lane + piece]
+            fp_copy(c, j, i).start()
+
+        def post(c, j, i, go=True):
+            sum_pair(c, j, i)
+
+            @pl.when((j == 0) & go)
+            def _():
+                fr_start(c, i)
+
+            @pl.when((j == 1) & (c < n_early))
+            def _():
+                back(c, i).start()
+
+            @pl.when((j == 1) & (c >= n_early))
+            def _():
+                for t in range(1, ny):
+                    fs_copy(c, i, t).start()
+
+        def units(c, j, go=True):
+            def one(n):
+                @pl.when(n < seqs)
                 def _():
-                    pump(early)
-
-        loop(0, seqs, partner_rows)
-        ready = min(early + 1, nc)
-        lag = 2
-
-        def chunk(c):
-            @pl.when((c + 1 >= ready) & (c + 1 < nc))
-            def _():
-                pump(c + 1)
-
-            complete("down", c)
-
-            def unit(n):
-                @pl.when(n < 2 * seqs)
-                def _():
-                    j, i = 1 - n // seqs, lax.rem(n, seqs)
-                    r = at(i, LEN)
-
-                    @pl.when(c >= 2)
-                    def _():
-                        fp_copy(c - 2, j, i).wait_send()
-
-                    product = dot(active[j, r, 0:hidden], down_w[c]).astype(BF16)
-                    for b in range(ny):
-                        for half in range(2):
-                            lane = (2 * b + half) * piece
-                            fpart[lax.rem(c, 2), j, b, half, r, :] = product[:, lane:lane + piece]
-                    fp_copy(c, j, i).start()
+                    unit(c, j, n)
 
                 @pl.when(n >= lag)
                 def _():
-                    m = n - lag
-                    j, i = 1 - m // seqs, lax.rem(m, seqs)
-                    sum_pair(c, j, i)
-
-                    @pl.when(j == 0)
-                    def _():
-                        fr_start(c, i)
-
-                    @pl.when(j == 1)
-                    def _():
-                        back(c, i).start()
-
-            loop(0, 2 * seqs + lag, unit)
-
-        loop(0, nc, chunk)
-
-    own_gain4 = gain4[:, at(tp, own)].astype(F32)
+                    post(c, j, n - lag, go)
+
+            with jax.named_scope("units"):
+                loop(0, seqs + lag, one)
+
+        def chunk(c):
+            with jax.named_scope("down_wait"):
+                complete("down", c)
+
+        def client(step):
+            @pl.when(step < seqs)
+            def _():
+                with jax.named_scope("hand_wait"):
+                    hand(step).wait_recv()
+                r = at(step, LEN)
+                big[1, r, at(tp, own)] = land[r, :]
+                ag_start(1, step)
+
+            @pl.when(step < n_early)
+            def _():
+                chunk(step)
+                units(step, 0, False)
+
+            @pl.when((step >= 1) & (step < seqs + 1))
+            def _():
+                with jax.named_scope("ag_pass1"):
+                    ag_pass(1, step - 1)
+
+            takes(reached + 2 * step, jnp.minimum(reached + 2 * step + 2, total))
+
+            @pl.when(step == seqs)
+            def _():
+                loop(0, n_early, lambda c: loop(0, seqs, lambda i: fr_start(c, i)))
+
+            @pl.when(step >= 2)
+            def _():
+                i = step - 2
+                with jax.named_scope("lift1"):
+                    lift(1, i)
+                with jax.named_scope("early"):
+                    loop(0, n_early, lambda c: unit(c, 1, i))
+                    loop(0, n_early, lambda c: post(c, 1, i))
+
+        reached = max(taken, 2 * (4 + nu + n_early - 1) + 3) if nc > 1 else taken
+        takes(taken, reached)
+        loop(0, seqs + 2, client)
+        takes(min(reached + 2 * (seqs + 2), total), total)
+
+        def gather(c, i):
+            r = at(i, LEN)
+            sums = fpair[1, c, y, r, :].astype(F32)
+            for t in range(1, ny):
+                fs_copy(c, i, t).wait_recv()
+                sums = sums + fsum[t - 1, c - n_early, r, :].astype(F32)
+            fpair[1, c, y, r, :] = sums.astype(BF16)
+            back_own(c, i).start()
+
+        def later(c):
+            chunk(c)
+            units(c, 1)
+
+            @pl.when(c > n_early)
+            def _():
+                with jax.named_scope("gather"):
+                    loop(0, seqs, lambda i: gather(c - 1, i))
+
+        loop(n_early, nc, later)
+        units(n_early, 0)
+        with jax.named_scope("gather"):
+            loop(0, seqs, lambda i: gather(nc - 1, i))
+        loop(n_early + 1, nc, lambda c: units(c, 0))
+        loop(0, nu, lambda j: drain("up", j))
+
+    own_gain4 = row(gain4[at(tp, own)])
 
     def close(step):
         @pl.when(step < seqs)
@@ -582,9 +743,15 @@
             r = at(step, LEN)
             parts = []
             for c in range(nc):
+                if c >= n_early:
+                    @pl.when(jnp.logical_not(worker))
+                    def _():
+                        back_own(c, step).wait_recv()
                 total = fpair[0, c, y, r, :].astype(F32)
                 for t in range(1, ny):
-                    fr_copy(c, step, t).wait_recv()
+                    @pl.when(worker | (c < n_early))
+                    def _():
+                        fr_copy(c, step, t).wait_recv()
                     total = total + frs[t - 1, c, r, :].astype(F32)
                 parts.append(total)
             total = parts[0] if nc == 1 else jnp.concatenate(parts, axis=1)
@@ -597,18 +764,16 @@
             scale = en_get(2, step - 1)
             result[r, :] = (resid[r, :].astype(F32) + acc[r, :] * scale * own_gain4).astype(BF16)
 
-    loop(0, seqs + 1, close)
-
-    for k in range(3):
-        drain("mix", k)
-    drain("out", 0)
-    loop(0, nu, lambda j: drain("up", j))
-    loop(0, nc, lambda j: drain("down", j))
+    with jax.named_scope("close"):
+        loop(0, seqs + 1, close)
+
+    with jax.named_scope("drain"):
+        loop(0, nc, lambda j: drain("down", j))
 
     def finish(i):
         for t in range(1, ny):
             rs_copy(i, t).wait_send()
-            loop(0, nc, lambda c: fr_copy(c, i, t).wait_send())
+            loop(0, jnp.where(worker, nc, n_early), lambda c: fr_copy(c, i, t).wait_send())
         for stage in range(3):
             for t in range(1, ntp):
                 en_copy(stage, i, t).wait_send()
@@ -618,14 +783,18 @@
             ag_drain(0, i)
             ag_drain(1, i)
             for j in range(2):
-                loop(max(nc - 2, 0), nc, lambda c: fp_copy(c, j, i).wait_send())
-            loop(0, nc, lambda c: back(c, i).wait_send())
+                loop(0, nc, lambda c: fp_copy(c, j, i).wait_send())
+            loop(0, n_early, lambda c: back(c, i).wait_send())
+            loop(n_early, nc, lambda c: back_own(c, i).wait_send())
+            for t in range(1, ny):
+                loop(n_early, nc, lambda c: fs_copy(c, i, t).wait_send())
 
         @pl.when(jnp.logical_not(worker))
         def _():
             hand(i).wait_send()
 
-    loop(0, seqs, finish)
+    with jax.named_scope("finish"):
+        loop(0, seqs, finish)
 
 
 def solution(mesh):
@@ -659,9 +828,10 @@
                 pltpu.VMEM((ny - 1, count, own), BF16),
                 pltpu.VMEM((count, own), F32),
                 pltpu.VMEM((count, own), BF16),
-                pltpu.VMEM((2, 2, ny, 2, count, piece), BF16),
+                pltpu.VMEM((nc, 2, ny, 2, count, piece), BF16),
                 pltpu.VMEM((2, nc, ny, count, piece), BF16),
                 pltpu.VMEM((ny - 1, nc, count, piece), BF16),
+                pltpu.VMEM((ny - 1, nc - early_chunks(nc), count, piece), BF16),
                 pltpu.VMEM((3, ntp, seqs, 8, LEN), F32),
                 dma((nk, nfs)), dma((nk, nfs)), dma((nk, nfs)), dma((nk, nfs)), dma((nk, nfs)),
                 dma((nk,)), dma,
@@ -669,12 +839,12 @@
                 dma((seqs, ny)), dma((seqs, ny)), dma((seqs, ny - 1)), dma((seqs, ny - 1)),
                 dma((3, seqs, ntp - 1)), dma((3, seqs, ntp - 1)),
                 dma((2, nc, seqs)), dma((2, nc, seqs)), dma((nc, seqs, ny - 1)), dma((nc, seqs, ny - 1)),
-                dma((nc, seqs)), dma((nc, seqs)),
+                dma((nc, seqs)), dma((nc, seqs)), dma((nc, seqs, ny - 1)), dma((nc, seqs, ny - 1)),
             ],
             compiler_params=pltpu.CompilerParams(
-                collective_id=0, has_side_effects=True, vmem_limit_bytes=66000000),
+                collective_id=0, has_side_effects=True, vmem_limit_bytes=67043328),
             name="layer",
-        )(tokens, gain1[None], wb, wc, wv, taps, wo, gain2[None], gain3[None], wu, wd, gain4[None])
+        )(tokens, gain1, wb, wc, wv, taps, wo, gain2, gain3, wu, wd, gain4)
 
     placed = (
         P(("rep", "fs"), "tp"), P(), P("fs", "tp"), P("fs", "tp"), P("fs", "tp"), P(), P("tp", "fs"),

time: 270 us -> 212 us (0.79)
  the two profiles are of different devices: /device:TPU:0 before, /device:TPU:9 now
where the time goes in v2:
time: 212 us
  Pallas kernels  209 us (99%)
  local copies, waits for them, and re-layouts  2.26 us (1%)
    pallas_call x1, Pallas kernels, body(): pl.pallas_call(functools.partial(kernel, nfs, ntp, nu, nc, cw), out_shape...  209 us

profile of v2, /device:TPU:9, one launch (start us, length us, event | category | flops | bytes accessed | tf_op | source)
XLA Modules:
  0.0 211.6 jit_solution(11477981422773701079)
XLA Ops:
  0.0 209.3 %layer.1 = bf16[1024,512]{1,0:T(8,128)(2,1)} custom-call(bf16[1024,512]{1,0:T(8,128)(2,1)} %tokens.1, bf16[2048]{0:T(1024)(128)(2,1)} %gain1.1, bf16[512,512]{1,0:T(8,128)(2,1)} %wb.1, bf16[512,512]{1,0:T(8,128)(2,1)} %wc.1, bf16[512,512]{1,0:T(8,128)(2,1)} %wv.1, bf16[3,2048]{1,0:T(4,128)(2,1)} %taps.1, bf16[512,512]{1,0:T(8,128)(2,1)} %wo.1, ...), custom_call_target="tpu_custom_call" | custom-call | tf_op jit(solution)/shard_map/layer/pallas_call | solution.py:815
  209.3 2.3 %copy.14 = bf16[1024,512]{1,0:T(8,128)(2,1)} copy(bf16[1024,512]{1,0:T(8,128)(2,1)} %layer.1) | data formatting | bytes 2097152

commit v3 on v2

--- a/solution.py
+++ b/solution.py
@@ -47,7 +47,7 @@
     result,
     rows_w, out_w, down_w, big, active, land, pair, rs, acc, resid, fpart, fpair, frs, fsum, energy,
     recv_z, recv_x, send_r, send_l, send_x, local_sem, tok_local,
-    ag_ys, ag_ds, ag_recv, land_send, land_recv,
+    ag_send, ag_recv, land_send, land_recv,
     pair_send, pair_recv, rs_send, rs_recv, en_send, en_recv,
     fp_send, fp_recv, fr_send, fr_recv, back_send, back_recv, fs_send, fs_recv,
 ):
@@ -64,6 +64,7 @@
     ocol = wo.shape[1]
     nk = 4 + nu + nc
     n_early = early_chunks(nc)
+    late = 4 + nu + min(2, nc)
     block = nfs * cw
     piece = block // ntp
     odd = lax.rem(fs, 2)
@@ -245,15 +246,15 @@
 
     def ag_y(j, i, t):
         src = tokens.at[at(i, LEN), :] if j == 2 else gathered(j, i, tp)
-        return group(up_y(t), src, gathered(j, i, tp), ag_ys.at[j, i, t - 1], ag_recv.at[j, i, tp])
+        return group(up_y(t), src, gathered(j, i, tp), ag_send.at[j], ag_recv.at[j, i, tp])
 
     def ag_pair(j, i):
         src = tokens.at[at(i, LEN), :] if j == 2 else gathered(j, i, tp)
-        return group(sibling, src, gathered(j, i, tp), ag_ds.at[j, i, 0], ag_recv.at[j, i, tp])
+        return group(sibling, src, gathered(j, i, tp), ag_send.at[j], ag_recv.at[j, i, tp])
 
     def ag_relay(j, i, t):
         who = down_y(t)
-        return group(sibling, gathered(j, i, who), gathered(j, i, who), ag_ds.at[j, i, t], ag_recv.at[j, i, who])
+        return group(sibling, gathered(j, i, who), gathered(j, i, who), ag_send.at[j], ag_recv.at[j, i, who])
 
     def ag_start(j, i):
         for t in range(1, ny):
@@ -268,13 +269,11 @@
     def ag_finish(j, i):
         for t in range(ny):
             who = lax.rem(y + t, ny) * 2 + 1 - core
-            group(sibling, gathered(j, i, who), gathered(j, i, who), ag_ds.at[j, i, 0], ag_recv.at[j, i, who]).wait_recv()
-
-    def ag_drain(j, i):
-        for t in range(1, ny):
-            ag_y(j, i, t).wait_send()
-            ag_relay(j, i, t).wait_send()
-        ag_pair(j, i).wait_send()
+            group(sibling, gathered(j, i, who), gathered(j, i, who), ag_send.at[j], ag_recv.at[j, i, who]).wait_recv()
+
+    def ag_drain(j):
+        sent = big.at[min(j, 1), :, 0:(2 * ny - 1) * own]
+        group(sibling, sent, sent, ag_send.at[j], ag_recv.at[j, 0, tp]).wait_send()
 
     def hand(i):
         return pltpu.make_async_remote_copy(
@@ -283,16 +282,16 @@
 
     def pair_copy(i, b):
         src = active.at[1, at(i, LEN), at(2 * b + 1 - core, own)]
-        return group(sibling, src, pair.at[b, at(i, LEN), :], pair_send.at[i, b], pair_recv.at[i, b])
+        return group(sibling, src, pair.at[b, at(i, LEN), :], pair_send, pair_recv.at[i, b])
 
     def rs_copy(i, t):
         src = pair.at[lax.rem(y + t, ny), at(i, LEN), :]
-        return group(up_y(t), src, rs.at[t - 1, at(i, LEN), :], rs_send.at[i, t - 1], rs_recv.at[i, t - 1])
+        return group(up_y(t), src, rs.at[t - 1, at(i, LEN), :], rs_send, rs_recv.at[i, t - 1])
 
     def en_copy(stage, i, t):
         return group(
             lax.rem(tp + t, ntp), energy.at[stage, 0, i], energy.at[stage, t, i],
-            en_send.at[stage, i, t - 1], en_recv.at[stage, i, t - 1])
+            en_send, en_recv.at[stage, i])
 
     def en_put(stage, i, values):
         square = jnp.sum(values * values, axis=1, keepdims=True)
@@ -302,8 +301,8 @@
             en_copy(stage, i, t).start()
 
     def en_get(stage, i):
-        for t in range(1, ntp):
-            en_copy(stage, i, t).wait_recv()
+        others = energy.at[stage, 1:ntp, i]
+        group(sibling, others, others, en_send, en_recv.at[stage, i]).wait_recv()
         flat = energy[stage, 0, i]
         for t in range(1, ntp):
             flat = flat + energy[stage, t, i]
@@ -313,15 +312,15 @@
     def fp_copy(c, j, i):
         return group(
             sibling, fpart.at[c, j, :, 1 - core, at(i, LEN), :], fpair.at[j, c, :, at(i, LEN), :],
-            fp_send.at[j, c, i], fp_recv.at[j, c, i])
+            fp_send, fp_recv.at[j, c, i])
 
     def fr_copy(c, i, t):
         src = fpair.at[0, c, lax.rem(y + t, ny), at(i, LEN), :]
-        return group(up_y(t), src, frs.at[t - 1, c, at(i, LEN), :], fr_send.at[c, i, t - 1], fr_recv.at[c, i, t - 1])
+        return group(up_y(t), src, frs.at[t - 1, c, at(i, LEN), :], fr_send, fr_recv.at[c, i, t - 1])
 
     def back(c, i):
         return pltpu.make_async_remote_copy(
-            fpair.at[1, c, :, at(i, LEN), :], fpair.at[0, c, :, at(i, LEN), :], back_send.at[c, i], back_recv.at[c, i],
+            fpair.at[1, c, :, at(i, LEN), :], fpair.at[0, c, :, at(i, LEN), :], back_send.at[0], back_recv.at[c, i],
             device_id={"fs": partner}, device_id_type=MESH)
 
     def send_at(k):
@@ -365,14 +364,17 @@
 
         @pl.when(lax.rem(q, 2) == 0)
         def _():
-            relay_at(q // 2, 1, 2, q == 0, True)
+            @pl.when(q // 2 < late)
+            def _():
+                relay_at(q // 2, 1, 2, q == 0, True)
+
             send_at(q // 2 + 2 + jnp.where(q >= 8, 1, 0))
 
             @pl.when(q == 6)
             def _():
                 send_at(6)
 
-            @pl.when(q >= 2)
+            @pl.when((q >= 2) & (q // 2 - 1 < late))
             def _():
                 relay_at(q // 2 - 1, 2, nfs, True, True)
 
@@ -398,11 +400,11 @@
     def fs_copy(c, i, t):
         src = fpair.at[1, c, lax.rem(y + t, ny), at(i, LEN), :]
         dst = fsum.at[t - 1, c - n_early, at(i, LEN), :]
-        return group(up_y(t), src, dst, fs_send.at[c, i, t - 1], fs_recv.at[c, i, t - 1])
+        return group(up_y(t), src, dst, fs_send, fs_recv.at[c, i, t - 1])
 
     def back_own(c, i):
         return pltpu.make_async_remote_copy(
-            fpair.at[1, c, y, at(i, LEN), :], fpair.at[0, c, y, at(i, LEN), :], back_send.at[c, i], back_recv.at[c, i],
+            fpair.at[1, c, y, at(i, LEN), :], fpair.at[0, c, y, at(i, LEN), :], back_send.at[1], back_recv.at[c, i],
             device_id={"fs": partner}, device_id_type=MESH)
 
     send_own("mix", 0)
@@ -448,7 +450,7 @@
     outer_mix((2, 2), (3, 1), (2, 3))
     send_outer(2, nu)
     outer_mix((3, 2), (3, 3))
-    send_outer(nu, nu + nc)
+    send_outer(nu, nu + min(2, nc))
     with jax.named_scope("mix_wait"):
         for k in range(3):
             complete("mix", k)
@@ -466,41 +468,58 @@
         outer = dot(rows, rows_w[0]).astype(BF16).astype(F32)
         active[0, r, 0:chan] = (outer * conv).astype(BF16)
 
-        @pl.when(i == seqs // 2)
-        def _():
-            takes(8, 9)
-
-    with jax.named_scope("mixer"):
-        loop(0, seqs, mixer)
-    takes(7, 8)
-    takes(9, 10)
-    with jax.named_scope("out_wait"):
-        complete("out", 0)
-
     def project(i):
         r = at(i, LEN)
-
-        @pl.when(i < seqs)
-        def _():
-            active[1, r, 0:width] = dot(active[0, r, 0:chan], out_w[...]).astype(BF16)
-            for b in range(ny):
-                pair_copy(i, b).start()
-
-        @pl.when(i > 0)
-        def _():
-            last = i - 1
-            r = at(last, LEN)
-            for b in range(ny):
-                pair_copy(last, b).wait_recv()
-                total = active[1, r, at(2 * b + core, own)].astype(F32) + pair[b, r, :].astype(F32)
-                pair[b, r, :] = total.astype(BF16)
-            for t in range(1, ny):
-                rs_copy(last, t).start()
-
-    with jax.named_scope("project"):
-        loop(0, seqs + 1, project)
+        active[1, r, 0:width] = dot(active[0, r, 0:chan], out_w[...]).astype(BF16)
+        for b in range(ny):
+            pair_copy(i, b).start()
+
+    def chip_sum(i):
+        r = at(i, LEN)
+        for b in range(ny):
+            pair_copy(i, b).wait_recv()
+            total = active[1, r, at(2 * b + core, own)].astype(F32) + pair[b, r, :].astype(F32)
+            pair[b, r, :] = total.astype(BF16)
+
+    def rs_start(i):
+        for t in range(1, ny):
+            rs_copy(i, t).start()
+
+    def mix(step):
+        @pl.when(step < seqs)
+        def _():
+            with jax.named_scope("mixer"):
+                mixer(step)
+
+        @pl.when(step == 1)
+        def _():
+            takes(8, 9)
+
+        @pl.when(step == 2)
+        def _():
+            takes(7, 8)
+            takes(9, 10)
+            with jax.named_scope("out_wait"):
+                complete("out", 0)
+
+        @pl.when((step >= 2) & (step < seqs + 2))
+        def _():
+            with jax.named_scope("project"):
+                project(step - 2)
+
+        @pl.when(step >= 3)
+        def _():
+            with jax.named_scope("chip_sum"):
+                chip_sum(step - 3)
+
+        @pl.when((step == 3) | (step == 4))
+        def _():
+            rs_start(step - 3)
+
+    loop(0, seqs + 3, mix)
     takes(10, 11)
-    loop(0, seqs, lambda i: ag_drain(2, i))
+    ag_drain(2)
+    group(sibling, active.at[1, :, 0:ny * own], active.at[1, :, 0:ny * own], pair_send, pair_recv.at[0, 0]).wait_send()
 
     own_gain2 = row(gain2[at(tp, own)])
     own_gain3 = row(gain3[at(tp, own)])
@@ -544,33 +563,35 @@
             active[j, r, pl.ds(u * ucol, ucol)] = (lifted * lifted).astype(BF16)
 
     def exchange(step):
-        @pl.when(step <= seqs)
-        def _():
-            takes(11 + step, 12 + step)
+        takes(11 + step, 12 + step)
 
         @pl.when(step < seqs)
         def _():
             with jax.named_scope("mixed_sum"):
                 mixed_sum(step)
-            for b in range(ny):
-                pair_copy(step, b).wait_send()
-
-        @pl.when((step >= seqs) & (step < 2 * seqs))
+
+        @pl.when((step >= 1) & (step < seqs + 1))
         def _():
             with jax.named_scope("add_resid"):
-                add_resid(step - seqs)
-
-        @pl.when(step >= 2 * seqs)
+                add_resid(step - 1)
+
+        @pl.when((step >= 2) & (step < seqs + 2))
         def _():
             with jax.named_scope("normalise"):
-                normalise(step - 2 * seqs)
+                normalise(step - 2)
+
+        @pl.when(step + 2 < seqs)
+        def _():
+            rs_start(step + 2)
 
         @pl.when(step < 3)
         def _():
             drain("mix", step)
 
     def spread(step):
-        takes(taken + step, taken + step + 1)
+        @pl.when(step < 3)
+        def _():
+            takes(taken + step, taken + step + 1)
 
         @pl.when(step < seqs)
         def _():
@@ -587,15 +608,16 @@
             with jax.named_scope("lift0"):
                 lift(0, step - 1)
 
-    loop(0, 3 * seqs, exchange)
-    taken = 12 + seqs
+    loop(0, max(seqs + 2, 3), exchange)
+    taken = 11 + max(seqs + 2, 3)
+    send_outer(nu + min(2, nc), nu + nc)
     drain("out", 0)
 
     @pl.when(worker)
     def _():
         loop(0, seqs + 1, spread)
 
-    taken += seqs + 1
+    taken += min(seqs + 1, 3)
 
     def sum_pair(c, j, i):
         r = at(i, LEN)
@@ -671,6 +693,14 @@
             with jax.named_scope("down_wait"):
                 complete("down", c)
 
+        def late_near(k):
+            with jax.named_scope("late"):
+                relay_at(k, 1, 2, False, True)
+
+        def late_far(k):
+            with jax.named_scope("late"):
+                relay_at(k, 2, nfs, True, True)
+
         def client(step):
             @pl.when(step < seqs)
             def _():
@@ -680,35 +710,54 @@
                 big[1, r, at(tp, own)] = land[r, :]
                 ag_start(1, step)
 
-            @pl.when(step < n_early)
-            def _():
-                chunk(step)
-                units(step, 0, False)
+            @pl.when((step == 0) & (n_early > 0))
+            def _():
+                chunk(0)
+                units(0, 0, False)
 
             @pl.when((step >= 1) & (step < seqs + 1))
             def _():
                 with jax.named_scope("ag_pass1"):
                     ag_pass(1, step - 1)
 
-            takes(reached + 2 * step, jnp.minimum(reached + 2 * step + 2, total))
-
-            @pl.when(step == seqs)
-            def _():
-                loop(0, n_early, lambda c: loop(0, seqs, lambda i: fr_start(c, i)))
+            takes(jnp.minimum(reached + step, total), jnp.minimum(reached + step + 1, total))
+
+            @pl.when((step >= 3) & (late + step - 3 < nk))
+            def _():
+                late_near(late + step - 3)
+
+            @pl.when((step >= 5) & (late + step - 5 < nk))
+            def _():
+                late_far(late + step - 5)
 
             @pl.when(step >= 2)
             def _():
                 i = step - 2
                 with jax.named_scope("lift1"):
                     lift(1, i)
+
+                @pl.when(step == 2)
+                def _():
+                    for c in range(1, n_early):
+                        chunk(c)
+
+                @pl.when(step == seqs)
+                def _():
+                    if n_early > 0:
+                        loop(0, seqs, lambda i: fr_start(0, i))
+
                 with jax.named_scope("early"):
                     loop(0, n_early, lambda c: unit(c, 1, i))
                     loop(0, n_early, lambda c: post(c, 1, i))
 
-        reached = max(taken, 2 * (4 + nu + n_early - 1) + 3) if nc > 1 else taken
+        reached = max(taken, 2 * (4 + nu) + 2 + n_early) if nc > 1 else taken
         takes(taken, reached)
         loop(0, seqs + 2, client)
-        takes(min(reached + 2 * (seqs + 2), total), total)
+        takes(min(reached + seqs + 2, total), total)
+        loop(min(late + seqs - 1, nk), nk, late_near)
+        loop(min(late + seqs - 3, nk), nk, late_far)
+        for c in range(1, n_early):
+            units(c, 0)
 
         def gather(c, i):
             r = at(i, LEN)
@@ -770,31 +819,29 @@
     with jax.named_scope("drain"):
         loop(0, nc, lambda j: drain("down", j))
 
-    def finish(i):
-        for t in range(1, ny):
-            rs_copy(i, t).wait_send()
-            loop(0, jnp.where(worker, nc, n_early), lambda c: fr_copy(c, i, t).wait_send())
-        for stage in range(3):
-            for t in range(1, ntp):
-                en_copy(stage, i, t).wait_send()
+    def sent(ref, sem):
+        group(sibling, ref, ref, sem, pair_recv.at[0, 0]).wait_send()
+
+    with jax.named_scope("finish"):
+        sent(rs, rs_send)
+        sent(energy.at[:, 1:ntp], en_send)
 
         @pl.when(worker)
         def _():
-            ag_drain(0, i)
-            ag_drain(1, i)
-            for j in range(2):
-                loop(0, nc, lambda c: fp_copy(c, j, i).wait_send())
-            loop(0, n_early, lambda c: back(c, i).wait_send())
-            loop(n_early, nc, lambda c: back_own(c, i).wait_send())
-            for t in range(1, ny):
-                loop(n_early, nc, lambda c: fs_copy(c, i, t).wait_send())
+            ag_drain(0)
+            ag_drain(1)
+            sent(fpair, fp_send)
+            sent(frs, fr_send)
+            sent(fsum, fs_send)
+            sent(fpair.at[1, n_early:nc, 0], back_send.at[1])
+            if n_early > 0:
+                sent(fpair.at[1, 0:n_early], back_send.at[0])
 
         @pl.when(jnp.logical_not(worker))
         def _():
-            hand(i).wait_send()
-
-    with jax.named_scope("finish"):
-        loop(0, seqs, finish)
+            if n_early > 0:
+                sent(frs.at[:, 0:n_early], fr_send)
+            loop(0, seqs, lambda i: hand(i).wait_send())
 
 
 def solution(mesh):
@@ -835,11 +882,11 @@
                 pltpu.VMEM((3, ntp, seqs, 8, LEN), F32),
                 dma((nk, nfs)), dma((nk, nfs)), dma((nk, nfs)), dma((nk, nfs)), dma((nk, nfs)),
                 dma((nk,)), dma,
-                dma((3, seqs, ny - 1)), dma((3, seqs, ny)), dma((3, seqs, ntp)), dma((seqs,)), dma((seqs,)),
-                dma((seqs, ny)), dma((seqs, ny)), dma((seqs, ny - 1)), dma((seqs, ny - 1)),
-                dma((3, seqs, ntp - 1)), dma((3, seqs, ntp - 1)),
-                dma((2, nc, seqs)), dma((2, nc, seqs)), dma((nc, seqs, ny - 1)), dma((nc, seqs, ny - 1)),
-                dma((nc, seqs)), dma((nc, seqs)), dma((nc, seqs, ny - 1)), dma((nc, seqs, ny - 1)),
+                dma((3,)), dma((3, seqs, ntp)), dma((seqs,)), dma((seqs,)),
+                dma, dma((seqs, ny)), dma, dma((seqs, ny - 1)),
+                dma, dma((3, seqs)),
+                dma, dma((2, nc, seqs)), dma, dma((nc, seqs, ny - 1)),
+                dma((2,)), dma((nc, seqs)), dma, dma((nc, seqs, ny - 1)),
             ],
             compiler_params=pltpu.CompilerParams(
                 collective_id=0, has_side_effects=True, vmem_limit_bytes=67043328),

time: 212 us -> 208 us (0.981)
  the two profiles are of different devices: /device:TPU:9 before, /device:TPU:0 now
where the time goes in v3:
time: 208 us; the launch traced here: 204 us
  Pallas kernels  202 us (97%)
  local copies, waits for them, and re-layouts  2.26 us (1%)
    pallas_call x1, Pallas kernels, body(): pl.pallas_call(functools.partial(kernel, nfs, ntp, nu, nc, cw), out_shape...  202 us

profile of v3, /device:TPU:0, one launch (start us, length us, event | category | flops | bytes accessed | tf_op | source)
XLA Modules:
  0.0 204.1 jit_solution(7932884963392407110)
XLA Ops:
  0.0 201.9 %layer.1 = bf16[1024,512]{1,0:T(8,128)(2,1)} custom-call(bf16[1024,512]{1,0:T(8,128)(2,1)} %tokens.1, bf16[2048]{0:T(1024)(128)(2,1)} %gain1.1, bf16[512,512]{1,0:T(8,128)(2,1)} %wb.1, bf16[512,512]{1,0:T(8,128)(2,1)} %wc.1, bf16[512,512]{1,0:T(8,128)(2,1)} %wv.1, bf16[3,2048]{1,0:T(4,128)(2,1)} %taps.1, bf16[512,512]{1,0:T(8,128)(2,1)} %wo.1, ...), custom_call_target="tpu_custom_call" | custom-call | tf_op jit(solution)/shard_map/layer/pallas_call | solution.py:862
  201.9 2.3 %copy.14 = bf16[1024,512]{1,0:T(8,128)(2,1)} copy(bf16[1024,512]{1,0:T(8,128)(2,1)} %layer.1) | data formatting | bytes 2097152

commit v4 on v3

--- a/solution.py
+++ b/solution.py
@@ -31,6 +31,10 @@
 
 def early_chunks(nc):
     return min(2, nc - 1)
+
+
+def direct_chunks(nc):
+    return min(3, nc - 1)
 
 
 def loop(low, high, fn):
@@ -64,6 +68,7 @@
     ocol = wo.shape[1]
     nk = 4 + nu + nc
     n_early = early_chunks(nc)
+    n_direct = direct_chunks(nc)
     late = 4 + nu + min(2, nc)
     block = nfs * cw
     piece = block // ntp
@@ -399,7 +404,7 @@
 
     def fs_copy(c, i, t):
         src = fpair.at[1, c, lax.rem(y + t, ny), at(i, LEN), :]
-        dst = fsum.at[t - 1, c - n_early, at(i, LEN), :]
+        dst = fsum.at[t - 1, c - n_direct, at(i, LEN), :]
         return group(up_y(t), src, dst, fs_send, fs_recv.at[c, i, t - 1])
 
     def back_own(c, i):
@@ -634,7 +639,7 @@
     def _():
         loop(0, nu, lambda j: drain("up", j))
 
-        frs[:, n_early:] = jnp.zeros((ny - 1, nc - n_early, count, piece), BF16)
+        frs[:, n_direct:] = jnp.zeros((ny - 1, nc - n_direct, count, piece), BF16)
 
         def returned(c):
             def one(i):
@@ -644,7 +649,7 @@
             loop(0, seqs, one)
 
         with jax.named_scope("returned"):
-            loop(0, n_early, returned)
+            loop(0, n_direct, returned)
 
     @pl.when(worker)
     def _():
@@ -667,11 +672,11 @@
             def _():
                 fr_start(c, i)
 
-            @pl.when((j == 1) & (c < n_early))
+            @pl.when((j == 1) & (c < n_direct))
             def _():
                 back(c, i).start()
 
-            @pl.when((j == 1) & (c >= n_early))
+            @pl.when((j == 1) & (c >= n_direct))
             def _():
                 for t in range(1, ny):
                     fs_copy(c, i, t).start()
@@ -756,32 +761,27 @@
         takes(min(reached + seqs + 2, total), total)
         loop(min(late + seqs - 1, nk), nk, late_near)
         loop(min(late + seqs - 3, nk), nk, late_far)
-        for c in range(1, n_early):
-            units(c, 0)
 
         def gather(c, i):
             r = at(i, LEN)
             sums = fpair[1, c, y, r, :].astype(F32)
             for t in range(1, ny):
                 fs_copy(c, i, t).wait_recv()
-                sums = sums + fsum[t - 1, c - n_early, r, :].astype(F32)
+                sums = sums + fsum[t - 1, c - n_direct, r, :].astype(F32)
             fpair[1, c, y, r, :] = sums.astype(BF16)
             back_own(c, i).start()
 
-        def later(c):
+        own_left = list(range(1, nc)) if n_early else list(range(nc))
+        while own_left and own_left[0] < n_early:
+            units(own_left.pop(0), 0)
+        for c in range(n_early, nc):
             chunk(c)
             units(c, 1)
-
-            @pl.when(c > n_early)
-            def _():
+        while own_left:
+            if len(own_left) == 1:
                 with jax.named_scope("gather"):
-                    loop(0, seqs, lambda i: gather(c - 1, i))
-
-        loop(n_early, nc, later)
-        units(n_early, 0)
-        with jax.named_scope("gather"):
-            loop(0, seqs, lambda i: gather(nc - 1, i))
-        loop(n_early + 1, nc, lambda c: units(c, 0))
+                    loop(n_direct, nc, lambda c: loop(0, seqs, lambda i: gather(c, i)))
+            units(own_left.pop(0), 0)
         loop(0, nu, lambda j: drain("up", j))
 
     own_gain4 = row(gain4[at(tp, own)])
@@ -792,13 +792,13 @@
             r = at(step, LEN)
             parts = []
             for c in range(nc):
-                if c >= n_early:
+                if c >= n_direct:
                     @pl.when(jnp.logical_not(worker))
                     def _():
                         back_own(c, step).wait_recv()
                 total = fpair[0, c, y, r, :].astype(F32)
                 for t in range(1, ny):
-                    @pl.when(worker | (c < n_early))
+                    @pl.when(worker | (c < n_direct))
                     def _():
                         fr_copy(c, step, t).wait_recv()
                     total = total + frs[t - 1, c, r, :].astype(F32)
@@ -833,14 +833,14 @@
             sent(fpair, fp_send)
             sent(frs, fr_send)
             sent(fsum, fs_send)
-            sent(fpair.at[1, n_early:nc, 0], back_send.at[1])
-            if n_early > 0:
-                sent(fpair.at[1, 0:n_early], back_send.at[0])
+            sent(fpair.at[1, n_direct:nc, 0], back_send.at[1])
+            if n_direct > 0:
+                sent(fpair.at[1, 0:n_direct], back_send.at[0])
 
         @pl.when(jnp.logical_not(worker))
         def _():
-            if n_early > 0:
-                sent(frs.at[:, 0:n_early], fr_send)
+            if n_direct > 0:
+                sent(frs.at[:, 0:n_direct], fr_send)
             loop(0, seqs, lambda i: hand(i).wait_send())
 
 
@@ -878,7 +878,7 @@
                 pltpu.VMEM((nc, 2, ny, 2, count, piece), BF16),
                 pltpu.VMEM((2, nc, ny, count, piece), BF16),
                 pltpu.VMEM((ny - 1, nc, count, piece), BF16),
-                pltpu.VMEM((ny - 1, nc - early_chunks(nc), count, piece), BF16),
+                pltpu.VMEM((ny - 1, nc - direct_chunks(nc), count, piece), BF16),
                 pltpu.VMEM((3, ntp, seqs, 8, LEN), F32),
                 dma((nk, nfs)), dma((nk, nfs)), dma((nk, nfs)), dma((nk, nfs)), dma((nk, nfs)),
                 dma((nk,)), dma,

time: 208 us -> 206 us (level)
  Pallas kernels: 202 us -> 199 us
    pallas_call x1, Pallas kernels: 202 us -> 199 us  [body(): pl.pallas_call(functools.partial(kernel, nfs, ntp, nu, nc, cw), out_shape...]
where the time goes in v4:
time: 206 us; the launch traced here: 201 us
  Pallas kernels  199 us (97%)
  local copies, waits for them, and re-layouts  2.26 us (1%)
    pallas_call x1, Pallas kernels, body(): pl.pallas_call(functools.partial(kernel, nfs, ntp, nu, nc, cw), out_shape...  199 us

profile of v4, /device:TPU:0, one launch (start us, length us, event | category | flops | bytes accessed | tf_op | source)
XLA Modules:
  0.0 201.4 jit_solution(3326027874588261359)
XLA Ops:
  0.0 199.2 %layer.1 = bf16[1024,512]{1,0:T(8,128)(2,1)} custom-call(bf16[1024,512]{1,0:T(8,128)(2,1)} %tokens.1, bf16[2048]{0:T(1024)(128)(2,1)} %gain1.1, bf16[512,512]{1,0:T(8,128)(2,1)} %wb.1, bf16[512,512]{1,0:T(8,128)(2,1)} %wc.1, bf16[512,512]{1,0:T(8,128)(2,1)} %wv.1, bf16[3,2048]{1,0:T(4,128)(2,1)} %taps.1, bf16[512,512]{1,0:T(8,128)(2,1)} %wo.1, ...), custom_call_target="tpu_custom_call" | custom-call | tf_op jit(solution)/shard_map/layer/pallas_call | solution.py:862
  199.2 2.3 %copy.14 = bf16[1024,512]{1,0:T(8,128)(2,1)} copy(bf16[1024,512]{1,0:T(8,128)(2,1)} %layer.1) | data formatting | bytes 2097152
